TPU v7x, 32 devices: a whole 2x2x4 slice. The times are simulated.
32 devices in a mesh: sp: 8 (over z, x), tp: 4 (over y, core).
Axes of the slice: x: 2, y: 2, z: 4, core: 2. Of those that a mesh axis runs over, the one named last changes fastest.
Arguments:
- latent: bfloat16 [4096, 2048], P(('sp', 'tp')), may hold values from -6 to 6
- context: bfloat16 [512, 2048], P('sp'), may hold values from -6 to 6
- conditioning: float32 [2048], P('sp'), may hold values from -6 to 6
- context_conditioning: float32 [2048], P('sp'), may hold values from -6 to 6
- shift_weight: bfloat16 [2048, 2048], P('sp', 'tp'), may hold values from -0.25 to 0.25
- scale_weight: bfloat16 [2048, 2048], P('sp', 'tp'), may hold values from -0.25 to 0.25
- gate_weight: bfloat16 [2048, 2048], P('sp', 'tp'), may hold values from -0.25 to 0.25
- norm_gain: float32 [2048], replicated, may hold values from 0.1 to 1.9
- query_weight: bfloat16 [2048, 2048], P(None, 'tp'), may hold values from -0.125 to 0.125
- key_weight: bfloat16 [2048, 1024], P(None, 'tp'), may hold values from -0.125 to 0.125
- value_weight: bfloat16 [2048, 1024], P(None, 'tp'), may hold values from -0.125 to 0.125
- query_gain: float32 [64], replicated, may hold values from 2 to 64, as said below
- key_gain: float32 [64], replicated, may hold values from 0.1 to 1.9
- context_lift: float32 [32], P('tp'), may hold values from 1.5 to 3
- output_weight: bfloat16 [2048, 2048], P('tp'), may hold values from -0.125 to 0.125
Outputs:
- mixed: bfloat16 [4096, 2048], P(('sp', 'tp'))
Inputs may be any that keep to these rules, and one draw needn't show every extreme that they name: `query_gain`: one gain for each channel of a head.
All inputs are finite; a program needn't handle non-finite values.
Results may differ from a plain program's by a relative error of at most 0.018.
The roundings to bfloat16 on the way count: a program that leaves them out, or rounds other values in their place, can miss the bound.
Values may be sent and summed in bfloat16 or wider, within the bound.
A program may use at most 128 MiB of HBM per device.

v0:
```python
import math
import jax
import jax.numpy as jnp
from jax import lax
from jax.sharding import PartitionSpec as P

HEAD = 64
GRID = 64
EPSILON = 1e-06
ROTARY_BASE = 10000.0


def normalize(values, gain):
    return values * lax.rsqrt(jnp.mean(values * values, axis=-1, keepdims=True) + EPSILON) * gain


def rotary_tables(offset, count):
    position = offset + jnp.arange(count, dtype=jnp.int32)
    grid_row = (position // GRID).astype(jnp.float32)
    grid_column = (position % GRID).astype(jnp.float32)
    quarter = HEAD // 4
    frequency = ROTARY_BASE ** (-jnp.arange(quarter, dtype=jnp.float32) / quarter)
    angles = jnp.concatenate(
        [grid_row[:, None] * frequency, grid_column[:, None] * frequency], axis=1
    )
    return (jnp.repeat(jnp.cos(angles), 2, axis=1), jnp.repeat(jnp.sin(angles), 2, axis=1))


def rotate(values, cos_table, sin_table):
    pairs = values.reshape(values.shape[:-1] + (HEAD // 2, 2))
    turned = jnp.stack([-pairs[..., 1], pairs[..., 0]], axis=-1).reshape(values.shape)
    return values * cos_table[:, None, :] + turned * sin_table[:, None, :]


def absorb(state, queries, keys, values, lift):
    top, total, weighted = state
    scores = (
        jnp.einsum("qkgd,skd->kgqs", queries, keys, preferred_element_type=jnp.float32)
        * HEAD ** (-0.5)
        + lift
    )
    new_top = jnp.maximum(top, jnp.max(scores, axis=-1))
    factor = jnp.exp(top - new_top)
    weights = jnp.exp(scores - new_top[..., None])
    total = total * factor + jnp.sum(weights, axis=-1)
    weighted = weighted * factor[..., None] + jnp.einsum(
        "kgqs,skd->kgqd", weights.astype(jnp.bfloat16), values, preferred_element_type=jnp.float32
    )
    return (new_top, total, weighted)


def shards(
    latent,
    context,
    conditioning,
    context_conditioning,
    shift_weight,
    scale_weight,
    gate_weight,
    norm_gain,
    query_weight,
    key_weight,
    value_weight,
    query_gain,
    key_gain,
    context_lift,
    output_weight,
):
    key_heads = key_weight.shape[1] // HEAD
    query_heads = query_weight.shape[1] // HEAD
    group = query_heads // key_heads
    key_width = key_heads * HEAD
    query_width = query_heads * HEAD
    signals = jnp.stack([jax.nn.silu(conditioning), jax.nn.silu(context_conditioning)]).astype(
        jnp.bfloat16
    )
    partial_terms = jnp.stack(
        [
            jnp.dot(signals, shift_weight, preferred_element_type=jnp.float32),
            jnp.dot(signals, scale_weight, preferred_element_type=jnp.float32),
            jnp.dot(signals, gate_weight, preferred_element_type=jnp.float32),
        ],
        axis=1,
    )
    summed = lax.psum(partial_terms, "sp")
    modulation = lax.all_gather(summed, "tp", axis=2, tiled=True)
    hidden = (
        normalize(latent.astype(jnp.float32), norm_gain) * (1.0 + modulation[0, 1])
        + modulation[0, 0]
    ).astype(jnp.bfloat16)
    piece = lax.all_gather(hidden, "tp", axis=0, tiled=True)
    projected = jnp.concatenate(
        [
            jnp.dot(piece, query_weight, preferred_element_type=jnp.float32),
            jnp.dot(piece, key_weight, preferred_element_type=jnp.float32),
            jnp.dot(piece, value_weight, preferred_element_type=jnp.float32),
        ],
        axis=1,
    )
    length = projected.shape[0]
    cos_table, sin_table = rotary_tables(lax.axis_index("sp") * length, length)
    queries = rotate(
        normalize(projected[:, :query_width].reshape(length, query_heads, HEAD), query_gain),
        cos_table,
        sin_table,
    )
    queries = queries.astype(jnp.bfloat16).reshape(length, key_heads, group, HEAD)
    keys = rotate(
        normalize(
            projected[:, query_width : query_width + key_width].reshape(length, key_heads, HEAD),
            key_gain,
        ),
        cos_table,
        sin_table,
    )
    values = projected[:, query_width + key_width :].astype(jnp.bfloat16)
    packed = jnp.concatenate([keys.astype(jnp.bfloat16).reshape(length, key_width), values], axis=1)
    context_hidden = (
        normalize(context.astype(jnp.float32), norm_gain) * (1.0 + modulation[1, 1])
        + modulation[1, 0]
    ).astype(jnp.bfloat16)
    context_count = context.shape[0]
    context_keys = normalize(
        jnp.dot(context_hidden, key_weight, preferred_element_type=jnp.float32).reshape(
            context_count, key_heads, HEAD
        ),
        key_gain,
    )
    context_values = jnp.dot(
        context_hidden, value_weight, preferred_element_type=jnp.float32
    ).astype(jnp.bfloat16)
    context_packed = lax.all_gather(
        jnp.concatenate(
            [context_keys.astype(jnp.bfloat16).reshape(context_count, key_width), context_values],
            axis=1,
        ),
        "sp",
        axis=0,
        tiled=True,
    )
    context_total = context_packed.shape[0]
    start_state = (
        jnp.full((key_heads, group, length), -jnp.inf, jnp.float32),
        jnp.zeros((key_heads, group, length), jnp.float32),
        jnp.zeros((key_heads, group, length, HEAD), jnp.float32),
    )
    lift = context_lift.reshape(key_heads, group, 1, 1)
    state = absorb(
        start_state,
        queries,
        context_packed[:, :key_width].reshape(context_total, key_heads, HEAD),
        context_packed[:, key_width:].reshape(context_total, key_heads, HEAD),
        lift,
    )
    piece = lax.all_gather(packed, "sp", axis=0, tiled=True)
    count = piece.shape[0]
    block = math.gcd(count, 2048)

    def one_block(index, inner):
        part = lax.dynamic_slice_in_dim(piece, index * block, block, 0)
        return absorb(
            inner,
            queries,
            part[:, :key_width].reshape(block, key_heads, HEAD),
            part[:, key_width:].reshape(block, key_heads, HEAD),
            0.0,
        )

    top, total, weighted = lax.fori_loop(0, count // block, one_block, state)
    attended = weighted / total[..., None]
    attended = (
        jnp.transpose(attended, (2, 0, 1, 3)).reshape(length, query_width).astype(jnp.bfloat16)
    )
    by_rows = lax.all_to_all(attended, "tp", split_axis=0, concat_axis=1, tiled=True)
    projection = jnp.dot(
        by_rows,
        lax.all_gather(output_weight, "tp", axis=0, tiled=True),
        preferred_element_type=jnp.float32,
    )
    return (latent.astype(jnp.float32) + modulation[0, 2] * projection).astype(jnp.bfloat16)


def solution(mesh):
    in_specs = (
        P(("sp", "tp"), None),
        P("sp", None),
        P("sp"),
        P("sp"),
        P("sp", "tp"),
        P("sp", "tp"),
        P("sp", "tp"),
        P(),
        P(None, "tp"),
        P(None, "tp"),
        P(None, "tp"),
        P(),
        P(),
        P("tp"),
        P("tp", None),
    )
    out_specs = P(("sp", "tp"), None)
    return jax.shard_map(shards, mesh=mesh, in_specs=in_specs, out_specs=out_specs, check_vma=False)
```

profile of v0, /device:TPU:0, one launch (start us, length us, event | category | flops | bytes accessed | tf_op | source)
XLA Modules:
  0.0 280.8 jit_solution(9180749674133689789)
XLA Ops:
  6.5 0.8 fusion.43
  7.4 0.7 fusion.44
  8.1 1.1 convolution_bitcast_fusion
  9.2 1.1 convolution_bitcast_fusion.1
  10.3 1.1 convolution_bitcast_fusion.2
  11.4 38.8 %psum.7 = f32[2,3,512]{2,0,1:T(2,128)S(1)} all-reduce(f32[2,3,512]{2,0,1:T(2,128)S(1)} %pad_maximum_fusion.5), channel_id=1, replica_groups=mesh['sp'=8,'tp'=4] {'sp'}, use_global_device_ids=true, to_apply=%region_0.1 | all-reduce | flops 3072 | bytes 24576 | tf_op jit(solution)/shard_map/psum | solution.py:85
  50.2 5.2 %all_gather.15 = f32[2,3,2048]{2,0,1:T(2,128)S(1)} all-gather(f32[2,3,512]{2,0,1:T(2,128)S(1)} %psum.7), channel_id=1, replica_groups=mesh['sp'=8,'tp'=4] {'tp'}, dimensions={2}, use_global_device_ids=true | all-gather | bytes 61440 | tf_op jit(solution)/shard_map/all_gather | solution.py:86
  55.4 0.6 fusion.49
  56.1 1.2 fusion.19
  57.3 2.1 fusion.23
  59.6 0.2 fusion.34
  59.9 0.1 mul.343
  60.1 0.1 mul.351
  60.2 0.8 mul.369
  60.9 0.7 mul.320
  61.7 17.7 %all-gather.4.cloned.1.call-done = bf16[512,2048]{1,0:T(8,128)(2,1)} async-done(((bf16[128,2048]{1,0:T(8,128)(2,1)}), bf16[512,2048]{1,0:T(8,128)(2,1)}) %all-gather.4.cloned.1.call-update) | async-done | bytes 2097168 | tf_op jit(solution)/shard_map/all_gather | solution.py:91
  79.4 2.6 bitcast_reduce_fusion.3
  82.1 0.3 reshape.187
  82.4 0.3 multiply_multiply_fusion.1
  82.7 0.4 slice_negate_fusion.1
  83.1 0.5 pad_maximum_fusion.1
  83.6 1.2 reshape.188
  84.7 1.2 fusion.30
  86.0 2.6 convolution_convert_fusion
  88.6 0.8 pad_maximum_fusion.2
  89.5 0.7 all-gather.8.cloned.1.call-update
  90.2 0.2 fusion.24
  90.4 1.6 fusion.50
  92.0 1.6 convolution_convert_fusion.1
  93.5 0.7 mul.348
  94.3 0.1 mul.316
  94.4 0.1 reduce_sum.68
  94.5 0.1 mul.317
  94.7 0.1 mul.318
  94.8 32.9 %all_gather.16 = bf16[512,512]{1,0:T(8,128)(2,1)S(1)} all-gather(bf16[64,512]{1,0:T(8,128)(2,1)S(1)} %pad_maximum_fusion.3), channel_id=1, replica_groups=mesh['sp'=8,'tp'=4] {'sp'}, dimensions={0}, use_global_device_ids=true | all-gather | bytes 589824 | tf_op jit(solution)/shard_map/all_gather | solution.py:132
  127.8 0.1 copy.43
  127.9 1.3 add.225
  129.3 0.8 copy.44
  130.1 3.6 %bitcast_reduce_fusion.2 = (f32[512,8]{0,1:T(8,128)}, f32[512,512]{0,1:T(8,128)S(1)}) fusion(bf16[512,2048]{1,0:T(8,128)(2,1)} %all-gather.4.cloned.1.call-done, bf16[2048,512]{1,0:T(8,128)(2,1)S(1)} %copy-done), kind=kOutput, calls=%fused_computation.35 | convolution fusion | flops 1074262016 | bytes 5259264 | tf_op jit(solution)/shard_map/dot_general | solution.py:94
  133.7 0.6 reshape.184
  134.3 0.7 add_rsqrt_fusion.1
  135.0 0.6 rsqrt.48
  135.7 1.2 multiply_multiply_fusion
  136.8 0.9 slice_negate_fusion
  137.7 1.9 pad_maximum_fusion
  139.6 2.0 reshape.185
  141.6 1.3 add_convert_fusion
  142.9 2.2 bitcast_reduce_fusion.1
  145.1 1.7 fusion.11
  146.9 2.4 fusion.16
  149.3 20.4 %all-gather.6.cloned.1.call-done = bf16[4096,512]{0,1:T(8,128)(2,1)} async-done(((bf16[512,512]{0,1:T(8,128)(2,1)}), bf16[4096,512]{0,1:T(8,128)(2,1)}) %all-gather.6.cloned.1.call-update) | async-done | bytes 4194320 | tf_op jit(solution)/shard_map/all_gather | solution.py:155
  169.7 87.2 %while.17 = (s32[]{:T(128)}, f32[4,2,512]{2,1,0:T(2,128)S(1)}, f32[4,2,512]{2,1,0:T(2,128)S(1)}, f32[4,2,512,64]{2,3,1,0:T(8,128)S(1)}, bf16[4096,512]{0,1:T(8,1...) while((s32[]{:T(128)}, f32[4,2,512]{2,1,0:T(2,128)S(1)}, ...), condition=%wide.region_11.12_spmd, body=%wide.region_8.11_spmd.sunk | while | flops 2215124992 | bytes 109838512 | solution.py:169
  169.7 1.8 fusion.81
  171.5 15.8 %bitcast_reduce_fusion.5 = (f32[4,2,512]{2,1,0:T(2,128)S(1)}, f32[4,2048,512,2]{2,1,3,0:T(8,128)}) fusion(bf16[2048,4,64,1]{0,2,3,1:T(8,128)(2,1)S(1)} %bitcast.152, bf16[512,4,2,64]{0,3,2,1:T(8,128)(2,1)S(1)} %get-tuple-element.242), kind=kOutput, calls=%fused_computation.1.clone.1 | convolution fusion | flops 1090514944 | bytes 35143680 | tf_op jit(solution)/shard_map/while/body/eval_jaxpr/qkgd,skd->kgqs/dot_general | solution.py:38
  187.3 13.7 %fusion.82 = f32[4,2,512]{2,1,0:T(2,128)S(1)} fusion(f32[4,2048,512,2]{2,1,3,0:T(8,128)} %get-tuple-element.211, f32[4,2,512]{2,1,0:T(2,128)S(1)} %max.8), kind=kLoop, calls=%fused_computation.4.clone.1 | loop fusion | flops 25161728 | bytes 33587200 | tf_op jit(solution)/shard_map/while/body/eval_jaxpr/reduce_sum | solution.py:45
  201.1 13.7 %fusion.83 = f32[4,2,512,64]{2,3,1,0:T(8,128)S(1)} fusion(bf16[2048,4,64,1]{0,2,3,1:T(8,128)(2,1)S(1)} %bitcast.153, f32[4,2048,512,2]{2,1,3,0:T(8,128)} %get-tuple-element.211, f32[4,2,512]{2,1,0:T(2,128)S(1)} %max.8, f32[4,2,512,64]{2,3,1,0:T(8,128)S(1)} %get-tuple-element.229, f32[4,2,512]{2,1,0:T(2,128)S(1)} %bitcast.159), kind=kOutput, calls=%fused_computation.6.clone.1 | convolution fusion | flops 1099431936 | bytes 36732928 | tf_op jit(solution)/shard_map/while/body/eval_jaxpr/kgqs,skd->kgqd/dot_general | solution.py:46
  214.8 1.7 fusion.81
  216.5 13.3 %bitcast_reduce_fusion.5 = (f32[4,2,512]{2,1,0:T(2,128)S(1)}, f32[4,2048,512,2]{2,1,3,0:T(8,128)}) fusion(bf16[2048,4,64,1]{0,2,3,1:T(8,128)(2,1)S(1)} %bitcast.152, bf16[512,4,2,64]{0,3,2,1:T(8,128)(2,1)S(1)} %get-tuple-element.242), kind=kOutput, calls=%fused_computation.1.clone.1 | convolution fusion | flops 1090514944 | bytes 35143680 | tf_op jit(solution)/shard_map/while/body/eval_jaxpr/qkgd,skd->kgqs/dot_general | solution.py:38
  229.8 13.6 %fusion.82 = f32[4,2,512]{2,1,0:T(2,128)S(1)} fusion(f32[4,2048,512,2]{2,1,3,0:T(8,128)} %get-tuple-element.211, f32[4,2,512]{2,1,0:T(2,128)S(1)} %max.8), kind=kLoop, calls=%fused_computation.4.clone.1 | loop fusion | flops 25161728 | bytes 33587200 | tf_op jit(solution)/shard_map/while/body/eval_jaxpr/reduce_sum | solution.py:45
  243.4 13.5 %fusion.83 = f32[4,2,512,64]{2,3,1,0:T(8,128)S(1)} fusion(bf16[2048,4,64,1]{0,2,3,1:T(8,128)(2,1)S(1)} %bitcast.153, f32[4,2048,512,2]{2,1,3,0:T(8,128)} %get-tuple-element.211, f32[4,2,512]{2,1,0:T(2,128)S(1)} %max.8, f32[4,2,512,64]{2,3,1,0:T(8,128)S(1)} %get-tuple-element.229, f32[4,2,512]{2,1,0:T(2,128)S(1)} %bitcast.159), kind=kOutput, calls=%fused_computation.6.clone.1 | convolution fusion | flops 1099431936 | bytes 36732928 | tf_op jit(solution)/shard_map/while/body/eval_jaxpr/kgqs,skd->kgqd/dot_general | solution.py:46
  256.9 0.1 fusion.32
  257.1 0.1 convert_element_type.83
  257.3 11.5 %all_to_all.16 = bf16[4,128,512]{1,2,0:T(8,128)(2,1)S(1)} all-to-all(bf16[4,128,512]{1,2,0:T(8,128)(2,1)S(1)} %copy.46), channel_id=1, replica_groups=mesh['sp'=8,'tp'=4] {'tp'}, dimensions={0} | all-to-all | bytes 1048576 | tf_op jit(solution)/shard_map/all_to_all | solution.py:174
  268.8 5.5 %fusion.15 = bf16[128,2048]{1,0:T(8,128)(2,1)} fusion(bf16[128,2048]{0,1:T(8,128)(2,1)S(1)} %bitcast.156, bf16[2048,2048]{1,0:T(8,128)(2,1)} %all-gather.8.cloned.1.call-done, bf16[128,2048]{1,0:T(8,128)(2,1)S(1)} %copy-done.2, f32[2048]{0:T(1024)S(1)} %bitcast.164), kind=kOutput, calls=%fused_computation.20 | convolution fusion | flops 1074790400 | bytes 9969664 | tf_op jit(solution)/shard_map/dot_general | solution.py:175
  (50 shorter events, 0.7 us)
Async XLA Ops:
  6.5 123.6 %copy-start = (bf16[2048,512]{1,0:T(8,128)(2,1)S(1)}, bf16[2048,512]{1,0:T(8,128)(2,1)}, u32[]{:S(2)}) copy-start(bf16[2048,512]{1,0:T(8,128)(2,1)} %param.25) | copy-start | bytes 6291460
  6.5 72.9 %all-gather.4.cloned.1.call-start = ((), (), s32[]{:S(2)}) async-start(), calls=%async_computation.1 | async-start | bytes 2621440 | tf_op jit(solution)/shard_map/all_gather | solution.py:91
  59.4 110.3 %all-gather.6.cloned.1.call-start = ((), (), s32[]{:S(2)}) async-start(), calls=%async_computation.2 | async-start | bytes 4718592 | tf_op jit(solution)/shard_map/all_gather | solution.py:155
  60.2 30.0 %copy-start.3 = (f32[512,64]{0,1:T(8,128)}, f32[512,64]{0,1:T(8,128)S(1)}, u32[]{:S(2)}) copy-start(f32[512,64]{0,1:T(8,128)S(1)} %mul.351) | copy-start | bytes 393220
  61.7 28.7 %copy-start.7 = (f32[2048]{0:T(1024)S(1)}, f32[2048]{0:T(1024)}, u32[]{:S(2)}) copy-start(f32[2048]{0:T(1024)} %param.24) | copy-start | bytes 24580
  82.4 11.1 %copy-start.9 = (f32[64]{0:T(128)S(1)}, f32[64]{0:T(128)}, u32[]{:S(2)}) copy-start(f32[64]{0:T(128)} %param.28) | copy-start | bytes 772
  84.7 5.5 %copy-start.4 = (bf16[64,2048]{1,0:T(8,128)(2,1)S(1)}, bf16[64,2048]{1,0:T(8,128)(2,1)}, u32[]{:S(2)}) copy-start(bf16[64,2048]{1,0:T(8,128)(2,1)} %param.18) | copy-start | bytes 786436
  89.5 179.3 %all-gather.8.cloned.1.call-start = ((), (), s32[]{:S(2)}) async-start(), calls=%async_computation.3 | async-start | bytes 10485760 | tf_op jit(solution)/shard_map/all_gather | solution.py:177
  141.6 3.5 %copy-start.6 = (f32[4,2]{1,0:T(4,128)S(1)}, f32[4,2]{1,0:T(4,128)}, u32[]{:S(2)}) copy-start(f32[4,2]{1,0:T(4,128)} %add.225) | copy-start | bytes 100
  142.9 4.0 %copy-start.5 = (bf16[512,256]{0,1:T(8,128)(2,1)S(1)}, bf16[512,256]{0,1:T(8,128)(2,1)}, u32[]{:S(2)}) copy-start(bf16[512,256]{0,1:T(8,128)(2,1)} %copy.44) | copy-start | bytes 786436
  169.7 99.1 %copy-start.2 = (bf16[128,2048]{1,0:T(8,128)(2,1)S(1)}, bf16[128,2048]{1,0:T(8,128)(2,1)}, u32[]{:S(2)}) copy-start(bf16[128,2048]{1,0:T(8,128)(2,1)} %param.17) | copy-start | bytes 1572868
  169.7 99.1 %copy-start.8 = (f32[1,1,2048]{2,0,1:T(1,128)S(1)}, f32[1,1,2048]{2,0,1:T(1,128)}, u32[]{:S(2)}) copy-start(f32[1,1,2048]{2,0,1:T(1,128)} %get-tuple-element.143) | copy-start | bytes 24580
  257.3 17.0 %copy-start.1 = (bf16[2048,512]{1,0:T(8,128)(2,1)S(1)}, bf16[2048,512]{1,0:T(8,128)(2,1)}, u32[]{:S(2)}) copy-start(bf16[2048,512]{1,0:T(8,128)(2,1)} %param.25) | copy-start | bytes 6291460
Sparse Core Ops, SparseCore 0:
  59.6 19.8 all-gather.3
  89.6 80.0 all-gather.5
  171.3 56.4 all-gather.7
where the time goes:
time: 282 us; the launch traced here: 281 us
  blocking collectives  88.5 us (31%)
  matrix products  81.5 us (29%)
  other arithmetic  44.6 us (16%)
  waiting for transfers between devices  38.9 us (14%)
  local copies, waits for them, and re-layouts  13.6 us (5%)
  between operations  13.5 us (5%)
    psum x1, blocking collectives, shards(): summed = lax.psum(partial_terms, 'sp')  38.8 us
    all_gather x1, blocking collectives, shards(): lax.all_gather(jnp.concatenate([context_keys.astype(jnp.bfloat16).reshape...  32.9 us
    dot_general x3, matrix products, absorb(): jnp.einsum('qkgd,skd->kgqs', queries, keys, preferred_element_type=jnp.fl...  31.3 us
    dot_general x3, matrix products, absorb(): jnp.einsum('kgqs,skd->kgqd', weights.astype(jnp.bfloat16), values, prefer...  29.6 us
    reduce_sum x3, other arithmetic, absorb(): total = total * factor + jnp.sum(weights, axis=-1)  29 us
    all_gather x1, waiting for transfers between devices, shards(): piece = lax.all_gather(packed, 'sp', axis=0, tiled=True)  20.4 us
    all_gather x1, waiting for transfers between devices, shards(): piece = lax.all_gather(hidden, 'tp', axis=0, tiled=True)  17.7 us
    all_to_all x1, blocking collectives, shards(): lax.all_to_all(attended, 'tp', split_axis=0, concat_axis=1, tiled=True)  11.5 us
  transfers between devices with their start and end apart: 3, of which 2 were waited for; matrix products, arithmetic and copies ran while one was open for 41% of the time, Pallas kernels for 0%

commit v1 on v0

--- a/solution.py
+++ b/solution.py
@@ -88,7 +88,13 @@
         normalize(latent.astype(jnp.float32), norm_gain) * (1.0 + modulation[0, 1])
         + modulation[0, 0]
     ).astype(jnp.bfloat16)
-    piece = lax.all_gather(hidden, "tp", axis=0, tiled=True)
+    n_dev = lax.axis_size("tp")
+    held, blocks = (hidden, [hidden])
+    for _ in range(n_dev - 1):
+        held = lax.ppermute(held, "tp", [(i, (i + 1) % n_dev) for i in range(n_dev)])
+        blocks.insert(0, held)
+    row_of_blocks = jnp.concatenate(blocks, axis=0)
+    piece = jnp.roll(row_of_blocks, (lax.axis_index("tp") + 1) * hidden.shape[0], axis=0)
     projected = jnp.concatenate(
         [
             jnp.dot(piece, query_weight, preferred_element_type=jnp.float32),

time: 282 us -> 291 us (1.032)
  local copies, waits for them, and re-layouts: 13.6 us -> 20.5 us
    ppermute x0 -> x3, waiting for transfers between devices: none -> 21.6 us  [shards(): lax.ppermute(held, 'tp', [(i, (i + 1) % n_dev) for i in range(n_dev)])]
    all_gather x1 -> x0, waiting for transfers between devices: 17.7 us -> none  [shards(): piece = lax.all_gather(hidden, 'tp', axis=0, tiled=True)]
    unnamed x20 -> x44, local copies, waits for them, and re-layouts: 0.04 us -> 6.12 us
  transfers between devices with their start and end apart: 3 -> 5, of which waited for: 2 -> 4; matrix products, arithmetic and copies ran while one was open for 41% -> 40% of each run, Pallas kernels for 0% -> 0%
where the time goes in v1:
time: 291 us; the launch traced here: 290 us
  blocking collectives  88.6 us (30%)
  matrix products  79.7 us (27%)
  other arithmetic  46.7 us (16%)
  waiting for transfers between devices  40.1 us (14%)
  local copies, waits for them, and re-layouts  20.5 us (7%)
  between operations  13.9 us (5%)
    psum x1, blocking collectives, shards(): summed = lax.psum(partial_terms, 'sp')  38.8 us
    all_gather x1, blocking collectives, shards(): lax.all_gather(jnp.concatenate([context_keys.astype(jnp.bfloat16).reshape...  33 us
    dot_general x3, matrix products, absorb(): jnp.einsum('qkgd,skd->kgqs', queries, keys, preferred_element_type=jnp.fl...  31.3 us
    dot_general x3, matrix products, absorb(): jnp.einsum('kgqs,skd->kgqd', weights.astype(jnp.bfloat16), values, prefer...  29.6 us
    reduce_sum x3, other arithmetic, absorb(): total = total * factor + jnp.sum(weights, axis=-1)  29 us
    ppermute x3, waiting for transfers between devices, shards(): lax.ppermute(held, 'tp', [(i, (i + 1) % n_dev) for i in range(n_dev)])  21.6 us
    all_gather x1, waiting for transfers between devices, shards(): piece = lax.all_gather(packed, 'sp', axis=0, tiled=True)  17.8 us
    all_to_all x1, blocking collectives, shards(): lax.all_to_all(attended, 'tp', split_axis=0, concat_axis=1, tiled=True)  11.5 us
  transfers between devices with their start and end apart: 5, of which 4 were waited for; matrix products, arithmetic and copies ran while one was open for 40% of the time, Pallas kernels for 0%

profile of v1, /device:TPU:0, one launch (start us, length us, event | category | flops | bytes accessed | tf_op | source)
XLA Modules:
  0.0 290.1 jit_solution(8988126137939520881)
XLA Ops:
  6.5 0.8 fusion.52
  7.4 0.7 fusion.53
  8.1 1.1 convolution_bitcast_fusion
  9.2 1.1 convolution_bitcast_fusion.1
  10.3 1.1 convolution_bitcast_fusion.2
  11.4 38.8 %psum.7 = f32[2,3,512]{2,0,1:T(2,128)S(1)} all-reduce(f32[2,3,512]{2,0,1:T(2,128)S(1)} %pad_maximum_fusion.5), channel_id=1, replica_groups=mesh['sp'=8,'tp'=4] {'sp'}, use_global_device_ids=true, to_apply=%region_0.1 | all-reduce | flops 3072 | bytes 24576 | tf_op jit(solution)/shard_map/psum | solution.py:85
  50.2 5.2 %all_gather.12 = f32[2,3,2048]{2,0,1:T(2,128)S(1)} all-gather(f32[2,3,512]{2,0,1:T(2,128)S(1)} %psum.7), channel_id=1, replica_groups=mesh['sp'=8,'tp'=4] {'tp'}, dimensions={2}, use_global_device_ids=true | all-gather | bytes 61440 | tf_op jit(solution)/shard_map/all_gather | solution.py:86
  55.4 0.6 fusion.61
  56.1 1.2 fusion.28
  57.3 0.5 copy-done.16
  57.9 1.3 fusion.32
  59.2 0.4 collective-permute-start
  59.6 8.3 %collective-permute-done = bf16[128,2048]{1,0:T(8,128)(2,1)S(1)} collective-permute-done((bf16[128,2048]{1,0:T(8,128)(2,1)S(1)}, bf16[128,2048]{1,0:T(8,128)(2,1)S(1)}, u32[]{:S(2)}, u32[]{:S(2)}) %collective-permute-start) | collective-permute-done | bytes 524320 | tf_op jit(solution)/shard_map/ppermute | solution.py:94
  67.8 1.4 mul.373
  69.2 7.3 %collective-permute-done.1 = bf16[128,2048]{1,0:T(8,128)(2,1)} collective-permute-done((bf16[128,2048]{1,0:T(8,128)(2,1)S(1)}, bf16[128,2048]{1,0:T(8,128)(2,1)}, u32[]{:S(2)}, u32[]{:S(2)}) %collective-permute-start.1) | collective-permute-done | bytes 524320 | tf_op jit(solution)/shard_map/ppermute | solution.py:94
  76.7 0.9 fusion.43
  77.7 0.9 broadcast_in_dim.13
  78.7 0.7 mul.323
  79.5 6.0 %collective-permute-done.2 = bf16[128,2048]{1,0:T(8,128)(2,1)} collective-permute-done((bf16[128,2048]{1,0:T(8,128)(2,1)}, bf16[128,2048]{1,0:T(8,128)(2,1)}, u32[]{:S(2)}, u32[]{:S(2)}) %collective-permute-start.2) | collective-permute-done | bytes 524320 | tf_op jit(solution)/shard_map/ppermute | solution.py:94
  85.5 1.1 constant_dynamic-update-slice_fusion.7
  86.5 1.1 constant_dynamic-update-slice_fusion.6
  87.7 1.4 constant_dynamic-update-slice_fusion.4
  89.0 1.1 constant_dynamic-update-slice_fusion.3
  90.1 1.1 constant_dynamic-update-slice_fusion.2
  91.2 1.0 constant_dynamic-update-slice_fusion
  92.3 0.8 bitcast_reduce_fusion.3
  93.0 1.1 copy-done.12
  94.8 0.4 slice_negate_fusion.1
  95.2 0.5 pad_maximum_fusion.1
  95.7 1.2 reshape.188
  96.9 2.6 fusion.25
  99.5 1.2 fusion.39
  100.7 0.8 pad_maximum_fusion.2
  101.6 0.7 all-gather.5.cloned.1.call-update
  102.5 1.6 fusion.62
  104.1 1.6 convolution_convert_fusion
  105.7 0.7 mul.352
  107.0 33.0 %all_gather.13 = bf16[512,512]{1,0:T(8,128)(2,1)S(1)} all-gather(bf16[64,512]{1,0:T(8,128)(2,1)S(1)} %pad_maximum_fusion.3), channel_id=1, replica_groups=mesh['sp'=8,'tp'=4] {'sp'}, dimensions={0}, use_global_device_ids=true | all-gather | bytes 589824 | tf_op jit(solution)/shard_map/all_gather | solution.py:138
  140.2 0.7 add.241
  140.9 0.9 copy.44
  141.7 3.5 %bitcast_reduce_fusion.2 = (f32[512,8]{0,1:T(8,128)}, f32[512,512]{0,1:T(8,128)S(1)}) fusion(bf16[2048,512]{1,0:T(8,128)(2,1)S(1)} %copy-done, bf16[1024,2048]{1,0:T(8,128)(2,1)} %copy-done.12, s32[]{:T(128)S(6)} %select_n.40), kind=kOutput, calls=%fused_computation.41 | convolution fusion | flops 1074262016 | bytes 5259268 | tf_op jit(solution)/shard_map/dot_general | solution.py:100
  145.3 0.6 reshape.184
  145.9 0.7 add_rsqrt_fusion.1
  146.6 0.6 rsqrt.48
  147.2 1.2 multiply_multiply_fusion
  148.4 0.9 slice_negate_fusion
  149.3 1.9 pad_maximum_fusion
  151.2 1.9 reshape.185
  153.2 1.3 add_convert_fusion
  154.5 2.2 bitcast_reduce_fusion.1
  156.7 1.7 fusion.11
  158.5 2.4 fusion.22
  160.8 17.8 %all-gather.3.cloned.1.call-done = bf16[4096,512]{0,1:T(8,128)(2,1)} async-done(((bf16[512,512]{0,1:T(8,128)(2,1)}), bf16[4096,512]{0,1:T(8,128)(2,1)}) %all-gather.3.cloned.1.call-update) | async-done | bytes 4194320 | tf_op jit(solution)/shard_map/all_gather | solution.py:161
  178.7 87.2 %while.17 = (s32[]{:T(128)}, f32[4,2,512]{2,1,0:T(2,128)S(1)}, f32[4,2,512]{2,1,0:T(2,128)S(1)}, f32[4,2,512,64]{2,3,1,0:T(8,128)S(1)}, bf16[4096,512]{0,1:T(8,1...) while((s32[]{:T(128)}, f32[4,2,512]{2,1,0:T(2,128)S(1)}, ...), condition=%wide.region_11.12_spmd, body=%wide.region_8.11_spmd.sunk | while | flops 2215124992 | bytes 109838512 | solution.py:175
  178.7 1.8 fusion.90
  180.5 15.8 %bitcast_reduce_fusion.5 = (f32[4,2,512]{2,1,0:T(2,128)S(1)}, f32[4,2048,512,2]{2,1,3,0:T(8,128)}) fusion(bf16[2048,4,64,1]{0,2,3,1:T(8,128)(2,1)S(1)} %bitcast.149, bf16[512,4,2,64]{0,3,2,1:T(8,128)(2,1)S(1)} %get-tuple-element.242), kind=kOutput, calls=%fused_computation.1.clone.1 | convolution fusion | flops 1090514944 | bytes 35143680 | tf_op jit(solution)/shard_map/while/body/eval_jaxpr/qkgd,skd->kgqs/dot_general | solution.py:38
  196.3 13.7 %fusion.91 = f32[4,2,512]{2,1,0:T(2,128)S(1)} fusion(f32[4,2048,512,2]{2,1,3,0:T(8,128)} %get-tuple-element.211, f32[4,2,512]{2,1,0:T(2,128)S(1)} %max.8), kind=kLoop, calls=%fused_computation.4.clone.1 | loop fusion | flops 25161728 | bytes 33587200 | tf_op jit(solution)/shard_map/while/body/eval_jaxpr/reduce_sum | solution.py:45
  210.0 13.7 %fusion.92 = f32[4,2,512,64]{2,3,1,0:T(8,128)S(1)} fusion(bf16[2048,4,64,1]{0,2,3,1:T(8,128)(2,1)S(1)} %bitcast.150, f32[4,2048,512,2]{2,1,3,0:T(8,128)} %get-tuple-element.211, f32[4,2,512]{2,1,0:T(2,128)S(1)} %max.8, f32[4,2,512,64]{2,3,1,0:T(8,128)S(1)} %get-tuple-element.229, f32[4,2,512]{2,1,0:T(2,128)S(1)} %bitcast.156), kind=kOutput, calls=%fused_computation.6.clone.1 | convolution fusion | flops 1099431936 | bytes 36732928 | tf_op jit(solution)/shard_map/while/body/eval_jaxpr/kgqs,skd->kgqd/dot_general | solution.py:46
  223.8 1.7 fusion.90
  225.5 13.3 %bitcast_reduce_fusion.5 = (f32[4,2,512]{2,1,0:T(2,128)S(1)}, f32[4,2048,512,2]{2,1,3,0:T(8,128)}) fusion(bf16[2048,4,64,1]{0,2,3,1:T(8,128)(2,1)S(1)} %bitcast.149, bf16[512,4,2,64]{0,3,2,1:T(8,128)(2,1)S(1)} %get-tuple-element.242), kind=kOutput, calls=%fused_computation.1.clone.1 | convolution fusion | flops 1090514944 | bytes 35143680 | tf_op jit(solution)/shard_map/while/body/eval_jaxpr/qkgd,skd->kgqs/dot_general | solution.py:38
  238.8 13.6 %fusion.91 = f32[4,2,512]{2,1,0:T(2,128)S(1)} fusion(f32[4,2048,512,2]{2,1,3,0:T(8,128)} %get-tuple-element.211, f32[4,2,512]{2,1,0:T(2,128)S(1)} %max.8), kind=kLoop, calls=%fused_computation.4.clone.1 | loop fusion | flops 25161728 | bytes 33587200 | tf_op jit(solution)/shard_map/while/body/eval_jaxpr/reduce_sum | solution.py:45
  252.4 13.5 %fusion.92 = f32[4,2,512,64]{2,3,1,0:T(8,128)S(1)} fusion(bf16[2048,4,64,1]{0,2,3,1:T(8,128)(2,1)S(1)} %bitcast.150, f32[4,2048,512,2]{2,1,3,0:T(8,128)} %get-tuple-element.211, f32[4,2,512]{2,1,0:T(2,128)S(1)} %max.8, f32[4,2,512,64]{2,3,1,0:T(8,128)S(1)} %get-tuple-element.229, f32[4,2,512]{2,1,0:T(2,128)S(1)} %bitcast.156), kind=kOutput, calls=%fused_computation.6.clone.1 | convolution fusion | flops 1099431936 | bytes 36732928 | tf_op jit(solution)/shard_map/while/body/eval_jaxpr/kgqs,skd->kgqd/dot_general | solution.py:46
  266.3 11.5 %all_to_all.16 = bf16[4,128,512]{1,2,0:T(8,128)(2,1)S(1)} all-to-all(bf16[4,128,512]{1,2,0:T(8,128)(2,1)S(1)} %copy.46), channel_id=1, replica_groups=mesh['sp'=8,'tp'=4] {'tp'}, dimensions={0} | all-to-all | bytes 1048576 | tf_op jit(solution)/shard_map/all_to_all | solution.py:180
  277.8 5.5 %fusion.15 = bf16[128,2048]{1,0:T(8,128)(2,1)} fusion(bf16[128,2048]{0,1:T(8,128)(2,1)S(1)} %bitcast.153, bf16[2048,2048]{1,0:T(8,128)(2,1)} %all-gather.5.cloned.1.call-done, bf16[128,2048]{1,0:T(8,128)(2,1)S(1)} %copy-done.3, f32[2048]{0:T(1024)S(1)} %bitcast.167), kind=kOutput, calls=%fused_computation.20 | convolution fusion | flops 1074790400 | bytes 9969664 | tf_op jit(solution)/shard_map/dot_general | solution.py:181
  (79 shorter events, 2.5 us)
Async XLA Ops:
  6.5 135.2 %copy-start = (bf16[2048,512]{1,0:T(8,128)(2,1)S(1)}, bf16[2048,512]{1,0:T(8,128)(2,1)}, u32[]{:S(2)}) copy-start(bf16[2048,512]{1,0:T(8,128)(2,1)} %param.25) | copy-start | bytes 6291460
  6.5 84.7 %copy-start.2 = (bf16[128,2048]{1,0:T(8,128)(2,1)S(1)}, bf16[128,2048]{1,0:T(8,128)(2,1)}, u32[]{:S(2)}) copy-start(bf16[128,2048]{1,0:T(8,128)(2,1)} %param.17) | copy-start | bytes 1572868
  6.5 84.7 %copy-start.8 = (f32[2048]{0:T(1024)S(1)}, f32[2048]{0:T(1024)}, u32[]{:S(2)}) copy-start(f32[2048]{0:T(1024)} %param.24) | copy-start | bytes 24580
  6.5 172.1 %all-gather.3.cloned.1.call-start = ((), (), s32[]{:S(2)}) async-start(), calls=%async_computation.1 | async-start | bytes 4718592 | tf_op jit(solution)/shard_map/all_gather | solution.py:161
  56.1 1.3 copy-start.9
  57.3 0.5 copy-start.16
  59.2 8.7 %collective-permute-start = (bf16[128,2048]{1,0:T(8,128)(2,1)S(1)}, bf16[128,2048]{1,0:T(8,128)(2,1)S(1)}, u32[]{:S(2)}, u32[]{:S(2)}) collective-permute-start(bf16[128,2048]{1,0:T(8,128)(2,1)S(1)} %fusion.32), channel_id=1, source_target_pairs={{0,1},{1,2},{2,3},{3,0},{4,5},{5,6},{6,7},{7,4},{8,9},{9,10},{10,1... | collective-permute-start | bytes 1572872 | tf_op jit(solution)/shard_map/ppermute | solution.py:94
  67.8 8.7 %collective-permute-start.1 = (bf16[128,2048]{1,0:T(8,128)(2,1)S(1)}, bf16[128,2048]{1,0:T(8,128)(2,1)}, u32[]{:S(2)}, u32[]{:S(2)}) collective-permute-start(bf16[128,2048]{1,0:T(8,128)(2,1)S(1)} %collective-permute-done), channel_id=1, source_target_pairs={{0,1},{1,2},{2,3},{3,0},{4,5},{5,6},{6,7},{7,4},{8,9},{9,10},{10,1... | collective-permute-start | bytes 1572872 | tf_op jit(solution)/shard_map/ppermute | solution.py:94
  76.5 8.9 %collective-permute-start.2 = (bf16[128,2048]{1,0:T(8,128)(2,1)}, bf16[128,2048]{1,0:T(8,128)(2,1)}, u32[]{:S(2)}, u32[]{:S(2)}) collective-permute-start(bf16[128,2048]{1,0:T(8,128)(2,1)} %collective-permute-done.1), channel_id=1, source_target_pairs={{0,1},{1,2},{2,3},{3,0},{4,5},{5,6},{6,7},{7,4},{8,9},{9,10},{10,1... | collective-permute-start | bytes 1572872 | tf_op jit(solution)/shard_map/ppermute | solution.py:94
  78.7 20.9 %copy-start.4 = (f32[512,64]{0,1:T(8,128)}, f32[512,64]{0,1:T(8,128)S(1)}, u32[]{:S(2)}) copy-start(f32[512,64]{0,1:T(8,128)S(1)} %mul.355) | copy-start | bytes 393220
  78.7 15.8 %copy-start.11 = (f32[32,2]{1,0:T(8,128)S(1)}, f32[32,2]{1,0:T(8,128)}, u32[]{:S(2)}) copy-start(f32[32,2]{1,0:T(8,128)} %mul.373) | copy-start | bytes 772
  79.5 12.7 %copy-start.5 = (bf16[2048,256]{1,0:T(8,128)(2,1)S(1)}, bf16[2048,256]{1,0:T(8,128)(2,1)}, u32[]{:S(2)}) copy-start(bf16[2048,256]{1,0:T(8,128)(2,1)} %param.26) | copy-start | bytes 3145732
  92.2 1.9 copy-start.12
  92.2 10.3 %copy-start.14 = (f32[1,1,2048]{2,0,1:T(1,128)S(1)}, f32[1,1,2048]{2,0,1:T(1,128)}, u32[]{:S(2)}) copy-start(f32[1,1,2048]{2,0,1:T(1,128)} %get-tuple-element.146) | copy-start | bytes 24580
  92.3 10.3 %copy-start.15 = (f32[1,1,2048]{2,0,1:T(1,128)S(1)}, f32[1,1,2048]{2,0,1:T(1,128)}, u32[]{:S(2)}) copy-start(f32[1,1,2048]{2,0,1:T(1,128)} %get-tuple-element.147) | copy-start | bytes 24580
  94.5 11.2 %copy-start.17 = (f32[64]{0:T(128)S(1)}, f32[64]{0:T(128)}, u32[]{:S(2)}) copy-start(f32[64]{0:T(128)} %param.28) | copy-start | bytes 772
  95.7 44.5 %copy-start.18 = (f32[8]{0:T(128)S(1)}, f32[8]{0:T(128)}, u32[]{:S(2)}) copy-start(f32[8]{0:T(128)} %param.30) | copy-start | bytes 100
  96.9 5.5 %copy-start.6 = (bf16[64,2048]{1,0:T(8,128)(2,1)S(1)}, bf16[64,2048]{1,0:T(8,128)(2,1)}, u32[]{:S(2)}) copy-start(bf16[64,2048]{1,0:T(8,128)(2,1)} %param.18) | copy-start | bytes 786436
  101.6 176.2 %all-gather.5.cloned.1.call-start = ((), (), s32[]{:S(2)}) async-start(), calls=%async_computation.2 | async-start | bytes 10485760 | tf_op jit(solution)/shard_map/all_gather | solution.py:183
  153.2 3.5 %copy-start.10 = (f32[4,2]{1,0:T(4,128)S(1)}, f32[4,2]{1,0:T(4,128)}, u32[]{:S(2)}) copy-start(f32[4,2]{1,0:T(4,128)} %add.241) | copy-start | bytes 100
  154.5 4.0 %copy-start.7 = (bf16[512,256]{0,1:T(8,128)(2,1)S(1)}, bf16[512,256]{0,1:T(8,128)(2,1)}, u32[]{:S(2)}) copy-start(bf16[512,256]{0,1:T(8,128)(2,1)} %copy.44) | copy-start | bytes 786436
  178.7 99.1 %copy-start.3 = (bf16[128,2048]{1,0:T(8,128)(2,1)S(1)}, bf16[128,2048]{1,0:T(8,128)(2,1)}, u32[]{:S(2)}) copy-start(bf16[128,2048]{1,0:T(8,128)(2,1)} %param.17) | copy-start | bytes 1572868
  178.7 99.1 %copy-start.13 = (f32[1,1,2048]{2,0,1:T(1,128)S(1)}, f32[1,1,2048]{2,0,1:T(1,128)}, u32[]{:S(2)}) copy-start(f32[1,1,2048]{2,0,1:T(1,128)} %get-tuple-element.143) | copy-start | bytes 24580
  266.3 17.0 %copy-start.1 = (bf16[2048,512]{1,0:T(8,128)(2,1)S(1)}, bf16[2048,512]{1,0:T(8,128)(2,1)}, u32[]{:S(2)}) copy-start(bf16[2048,512]{1,0:T(8,128)(2,1)} %param.25) | copy-start | bytes 6291460
Sparse Core Ops, SparseCore 0:
  101.7 76.9 all-gather.2
  180.2 56.4 all-gather.4
